TPU v7x, 32 devices: a whole 2x2x4 slice. The times are simulated.
32 devices in a mesh: sp: 16 (over z, y, core), tp: 2 (over x).
Axes of the slice: x: 2, y: 2, z: 4, core: 2. Of those that a mesh axis runs over, the one named last changes fastest.
Arguments:
- queries: bfloat16 [3072, 1024], P('sp', 'tp'), may hold values from -6 to 6
- keys: bfloat16 [3072, 512], P('sp', 'tp'), may hold values from -6 to 6
- values: bfloat16 [3072, 512], P('sp', 'tp'), may hold values from -6 to 6
- q_gain: float32 [64], replicated, may hold values from 0.1 to 6.5
- k_gain: float32 [64], replicated, may hold values from 0.1 to 6.5
- w_out: bfloat16 [1024, 2048], P('tp'), may hold values from -12 to 12
- residual: bfloat16 [3072, 2048], P(('sp', 'tp')), may hold values from -6 to 6
- norm_gain: float32 [2048], replicated, may hold values from 0.1 to 1.9
- w_gate: bfloat16 [2048, 5632], P('sp', 'tp'), may hold values from -0.125 to 0.125
- w_up: bfloat16 [2048, 5632], P('sp', 'tp'), may hold values from -0.125 to 0.125
- w_down: bfloat16 [5632, 2048], P('tp', 'sp'), may hold values from -0.25 to 0.25
Outputs:
- layer_out: bfloat16 [3072, 2048], P(('sp', 'tp'))
All inputs are finite; a program needn't handle non-finite values.
Results may differ from a plain program's by a relative error of at most 0.018.
The roundings to bfloat16 on the way count: a program that leaves them out, or rounds other values in their place, can miss the bound.
Values may be sent and summed in bfloat16 or wider, within the bound.
A program may use at most 128 MiB of HBM per device.

v0:
```python
import math
import jax
import jax.numpy as jnp
from jax import lax
from jax.sharding import PartitionSpec as P

GRID_W = 128
EPS = 1e-06
THETA = 10000.0


def turn_half(part, angle):
    quarter = part.shape[-1] // 2
    cos_table = jnp.cos(angle)[:, None, :]
    sin_table = jnp.sin(angle)[:, None, :]
    first_part = part[..., :quarter]
    second_part = part[..., quarter:]
    return jnp.concatenate(
        [
            first_part * cos_table - second_part * sin_table,
            first_part * sin_table + second_part * cos_table,
        ],
        axis=-1,
    )


def head_norm_rope(flat, gain, offset, head_count):
    tok_rows = flat.shape[0]
    head_size = flat.shape[1] // head_count
    heads = flat.astype(jnp.float32).reshape(tok_rows, head_count, head_size)
    heads = heads * lax.rsqrt(jnp.mean(heads * heads, axis=-1, keepdims=True) + EPS) * gain
    positions = offset + jnp.arange(tok_rows, dtype=jnp.int32)
    row_pos = (positions // GRID_W).astype(jnp.float32)
    col_pos = (positions % GRID_W).astype(jnp.float32)
    half_size = head_size // 2
    inv_freq = THETA ** (-jnp.arange(0, half_size, 2, dtype=jnp.float32) / half_size)
    turned = jnp.concatenate(
        [
            turn_half(heads[..., :half_size], row_pos[:, None] * inv_freq[None, :]),
            turn_half(heads[..., half_size:], col_pos[:, None] * inv_freq[None, :]),
        ],
        axis=-1,
    )
    return turned.reshape(tok_rows, head_count * head_size).astype(jnp.bfloat16)


def body(queries, keys, values, q_gain, k_gain, w_out, residual, norm_gain, w_gate, w_up, w_down):
    tok_rows = queries.shape[0]
    head_size = q_gain.shape[0]
    q_heads = queries.shape[1] // head_size
    kv_heads = keys.shape[1] // head_size
    q_group = q_heads // kv_heads
    offset = lax.axis_index("sp") * tok_rows
    q_rot = head_norm_rope(queries, q_gain, offset, q_heads)
    k_rot = head_norm_rope(keys, k_gain, offset, kv_heads)
    query_groups = q_rot.reshape(tok_rows, kv_heads, q_group, head_size)
    score_scale = head_size ** (-0.5)
    start_state = (
        jnp.full((kv_heads, q_group, tok_rows), -1e30, jnp.float32),
        jnp.zeros((kv_heads, q_group, tok_rows), jnp.float32),
        jnp.zeros((kv_heads, q_group, tok_rows, head_size), jnp.float32),
    )
    running = start_state
    key_piece = lax.all_gather(k_rot, "sp", axis=0, tiled=True)
    value_piece = lax.all_gather(values, "sp", axis=0, tiled=True)
    piece_len = key_piece.shape[0]
    block_len = math.gcd(piece_len, 512)
    blocks = piece_len // block_len
    key_blocks = key_piece.reshape(blocks, block_len, kv_heads, head_size)
    value_blocks = value_piece.reshape(blocks, block_len, kv_heads, head_size)

    def update(state, block_pair):
        prior_max, totals, accum = state
        key_block, value_block = block_pair
        scores = (
            jnp.einsum(
                "qhgd,khd->hgqk", query_groups, key_block, preferred_element_type=jnp.float32
            )
            * score_scale
        )
        new_max = jnp.maximum(prior_max, jnp.max(scores, axis=-1))
        weights = jnp.exp(scores - new_max[..., None])
        factor = jnp.exp(prior_max - new_max)
        totals = totals * factor + jnp.sum(weights, axis=-1)
        accum = accum * factor[..., None] + jnp.einsum(
            "hgqk,khd->hgqd",
            weights.astype(jnp.bfloat16),
            value_block,
            preferred_element_type=jnp.float32,
        )
        return ((new_max, totals, accum), None)

    running, unused = lax.scan(update, running, (key_blocks, value_blocks))
    final_max, totals, accum = running
    mixed = accum / totals[..., None]
    attn = (
        jnp.transpose(mixed, (2, 0, 1, 3))
        .reshape(tok_rows, q_heads * head_size)
        .astype(jnp.bfloat16)
    )
    own_rows = lax.all_to_all(attn, "tp", split_axis=0, concat_axis=1, tiled=True)
    columns = own_rows
    proj = jnp.dot(
        columns, lax.all_gather(w_out, "tp", axis=0, tiled=True), preferred_element_type=jnp.float32
    )
    mid = residual.astype(jnp.float32) + proj
    normed = (
        mid * lax.rsqrt(jnp.mean(mid * mid, axis=-1, keepdims=True) + EPS) * norm_gain
    ).astype(jnp.bfloat16)
    gathered = lax.all_gather(normed, "tp", axis=0, tiled=True)
    columns = gathered
    gate = jnp.dot(
        columns,
        lax.all_gather(w_gate, "sp", axis=0, tiled=True),
        preferred_element_type=jnp.float32,
    )
    up_part = jnp.dot(
        columns, lax.all_gather(w_up, "sp", axis=0, tiled=True), preferred_element_type=jnp.float32
    )
    hidden = (jax.nn.silu(gate) * up_part).astype(jnp.bfloat16)
    terms = jnp.dot(
        hidden, lax.all_gather(w_down, "sp", axis=1, tiled=True), preferred_element_type=jnp.float32
    )
    down = lax.psum_scatter(
        terms.astype(jnp.bfloat16), "tp", scatter_dimension=0, tiled=True
    ).astype(jnp.float32)
    return (mid + 0.5 * down).astype(jnp.bfloat16)


def solution(mesh):
    return jax.shard_map(
        body,
        mesh=mesh,
        in_specs=(
            P("sp", "tp"),
            P("sp", "tp"),
            P("sp", "tp"),
            P(),
            P(),
            P("tp", None),
            P(("sp", "tp"), None),
            P(),
            P("sp", "tp"),
            P("sp", "tp"),
            P("tp", "sp"),
        ),
        out_specs=P(("sp", "tp"), None),
        check_vma=False,
    )
```

profile of v0, /device:TPU:0, one launch (start us, length us, event | category | flops | bytes accessed | tf_op | source)
XLA Modules:
  0.0 477.9 jit_solution(934830852998414411)
XLA Ops:
  6.6 1.0 copy.23
  13.3 38.7 %all-gather.7.cloned.1.call-done = bf16[3072,256]{1,0:T(8,128)(2,1)} async-done(((bf16[192,256]{1,0:T(8,128)(2,1)}), bf16[3072,256]{1,0:T(8,128)(2,1)}) %all-gather.7.cloned.1.call-update) | async-done | bytes 1572880 | tf_op jit(solution)/shard_map/all_gather | solution.py:64
  52.0 4.6 reshape.207
  56.6 3.3 copy.28
  59.9 32.7 %all-gather.9.cloned.1.call-done = bf16[3072,256]{1,0:T(8,128)(2,1)} async-done(((bf16[192,256]{1,0:T(8,128)(2,1)}), bf16[3072,256]{1,0:T(8,128)(2,1)}) %all-gather.9.cloned.1.call-update) | async-done | bytes 1572880 | tf_op jit(solution)/shard_map/all_gather | solution.py:65
  92.6 4.6 reshape.208
  97.2 3.3 copy.29
  100.5 32.2 %while.15 = (s32[]{:T(128)}, f32[4,2,192]{2,1,0:T(2,128)S(1)}, f32[4,2,192]{2,1,0:T(2,128)S(1)}, f32[4,2,192,64]{2,3,1,0:T(8,128)}, bf16[6,512,4,64]{1,3,2,0:T(8...) while((s32[]{:T(128)}, f32[4,2,192]{2,1,0:T(2,128)S(1)}, ...), condition=%wide.region_5.6_spmd.clone, body=%wide.region_2.5_spmd.clone.sunk | while | flops 207920640 | bytes 14189729 | solution.py:93
  100.5 1.7 bitcast_reduce_fusion.2
  103.4 1.8 fusion.52
  106.0 1.7 bitcast_reduce_fusion.2
  108.7 1.8 fusion.52
  111.4 1.7 bitcast_reduce_fusion.2
  114.1 1.8 fusion.52
  116.7 1.7 bitcast_reduce_fusion.2
  119.4 1.8 fusion.52
  122.1 1.7 bitcast_reduce_fusion.2
  124.8 1.8 fusion.52
  127.4 1.7 bitcast_reduce_fusion.2
  130.2 1.8 fusion.52
  132.8 1.1 fusion.25
  134.2 10.3 %all_to_all.16 = bf16[2,96,512]{2,1,0:T(8,128)(2,1)S(1)} all-to-all(bf16[2,96,512]{2,1,0:T(8,128)(2,1)S(1)} %copy.30), channel_id=1, replica_groups=mesh['sp'=16,'tp'=2] {'tp'}, dimensions={0} | all-to-all | bytes 393216 | tf_op jit(solution)/shard_map/all_to_all | solution.py:101
  144.5 7.2 %all-gather.11.cloned.1.call-done = bf16[1024,2048]{1,0:T(8,128)(2,1)} async-done(((bf16[512,2048]{1,0:T(8,128)(2,1)}), bf16[1024,2048]{1,0:T(8,128)(2,1)}) %all-gather.11.cloned.1.call-update) | async-done | bytes 4194320 | tf_op jit(solution)/shard_map/all_gather | solution.py:104
  151.7 3.2 multiply_reduce_fusion
  155.1 11.5 %all_gather.24 = bf16[192,2048]{1,0:T(8,128)(2,1)S(1)} all-gather(bf16[96,2048]{1,0:T(8,128)(2,1)S(1)} %multiply_convert_fusion), channel_id=1, replica_groups=mesh['sp'=16,'tp'=2] {'tp'}, dimensions={0}, use_global_device_ids=true | all-gather | bytes 1179648 | tf_op jit(solution)/shard_map/all_gather | solution.py:110
  166.6 81.3 %all-gather.13.cloned.1.call-done = bf16[2048,2816]{1,0:T(8,128)(2,1)} async-done(((bf16[128,2816]{1,0:T(8,128)(2,1)}), bf16[2048,2816]{1,0:T(8,128)(2,1)}) %all-gather.13.cloned.1.call-update) | async-done | bytes 11534352 | tf_op jit(solution)/shard_map/all_gather | solution.py:114
  247.9 8.0 %fusion.30 = f32[192,2816]{1,0:T(8,128)} fusion(bf16[192,2048]{1,0:T(8,128)(2,1)S(1)} %all_gather.24, bf16[2048,2816]{1,0:T(8,128)(2,1)} %all-gather.13.cloned.1.call-done), kind=kOutput, calls=%fused_computation.69 | convolution fusion | flops 2214592512 | bytes 14483456 | tf_op jit(solution)/shard_map/dot_general | solution.py:112
  255.9 86.4 %all-gather.15.cloned.1.call-done = bf16[2048,2816]{1,0:T(8,128)(2,1)} async-done(((bf16[128,2816]{1,0:T(8,128)(2,1)}), bf16[2048,2816]{1,0:T(8,128)(2,1)}) %all-gather.15.cloned.1.call-update) | async-done | bytes 11534352 | tf_op jit(solution)/shard_map/all_gather | solution.py:118
  342.3 97.2 %all-gather.17.cloned.1.call-done = bf16[2816,2048]{1,0:T(8,128)(2,1)} async-done(((bf16[2816,128]{1,0:T(8,128)(2,1)}), bf16[2816,2048]{1,0:T(8,128)(2,1)}) %all-gather.17.cloned.1.call-update) | async-done | bytes 11534352 | tf_op jit(solution)/shard_map/all_gather | solution.py:122
  439.4 13.9 %convolution_convert_fusion = bf16[192,2048]{1,0:T(8,128)(2,1)} fusion(bf16[2816,2048]{1,0:T(8,128)(2,1)} %all-gather.17.cloned.1.call-done, bf16[192,2048]{1,0:T(8,128)(2,1)S(1)} %all_gather.24, bf16[2048,2816]{1,0:T(8,128)(2,1)} %all-gather.15.cloned.1.call-done, f32[192,2816]{1,0:T(8,128)} %fusion.30), kind=kOutput, calls=%fused_computation.25 | convolution fusion | flops 4432822272 | bytes 26804224 | tf_op jit(solution)/shard_map/dot_general | solution.py:121
  453.3 15.8 %reduce-scatter.2.cloned.1.call-done = bf16[96,2048]{1,0:T(8,128)(2,1)} async-done(((bf16[192,2048]{1,0:T(8,128)(2,1)}), bf16[96,2048]{1,0:T(8,128)(2,1)}) %reduce-scatter.2.cloned.1.call-update) | async-done | bytes 393232 | tf_op jit(solution)/shard_map/reduce_scatter | solution.py:124
  469.2 1.8 add_convert_fusion
  (91 shorter events, 17.0 us)
Async XLA Ops:
  6.5 6.3 %copy-start.2 = (bf16[192,512]{1,0:T(8,128)(2,1)S(1)}, bf16[192,512]{1,0:T(8,128)(2,1)}, u32[]{:S(2)}) copy-start(bf16[192,512]{1,0:T(8,128)(2,1)} %param.13) | copy-start | bytes 589828
  6.5 45.4 %all-gather.7.cloned.1.call-start = ((), (), s32[]{:S(2)}) async-start(), calls=%async_computation.2 | async-start | bytes 1671168 | tf_op jit(solution)/shard_map/all_gather | solution.py:64
  8.4 4.6 copy-start.4
  9.5 83.1 %all-gather.9.cloned.1.call-start = ((), (), s32[]{:S(2)}) async-start(), calls=%async_computation.3 | async-start | bytes 1671168 | tf_op jit(solution)/shard_map/all_gather | solution.py:65
  10.2 141.5 %all-gather.11.cloned.1.call-start = ((), (), s32[]{:S(2)}) async-start(), calls=%async_computation.4 | async-start | bytes 6291456 | tf_op jit(solution)/shard_map/all_gather | solution.py:104
  11.0 236.9 %all-gather.13.cloned.1.call-start = ((), (), s32[]{:S(2)}) async-start(), calls=%async_computation.5 | async-start | bytes 12255232 | tf_op jit(solution)/shard_map/all_gather | solution.py:114
  11.6 330.7 %all-gather.15.cloned.1.call-start = ((), (), s32[]{:S(2)}) async-start(), calls=%async_computation.6 | async-start | bytes 12255232 | tf_op jit(solution)/shard_map/all_gather | solution.py:118
  12.1 427.3 %all-gather.17.cloned.1.call-start = ((), (), s32[]{:S(2)}) async-start(), calls=%async_computation.7 | async-start | bytes 12255232 | tf_op jit(solution)/shard_map/all_gather | solution.py:122
  12.7 456.4 %reduce-scatter.2.cloned.1.call-start = ((), (), s32[]{:S(2)}) async-start(), calls=%async_computation.8 | async-start | bytes 1179648 | tf_op jit(solution)/shard_map/reduce_scatter | solution.py:124
  102.3 1.1 copy-start
  105.2 0.8 copy-start.1
  107.7 1.0 copy-start
  110.5 0.8 copy-start.1
  113.0 1.0 copy-start
  115.9 0.8 copy-start.1
  118.4 1.0 copy-start
  121.2 0.8 copy-start.1
  123.8 1.0 copy-start
  126.6 0.8 copy-start.1
  129.1 1.0 copy-start
  132.0 0.8 copy-start.1
  134.2 20.7 %copy-start.3 = (f32[2048]{0:T(1024)S(1)}, f32[2048]{0:T(1024)}, u32[]{:S(2)}) copy-start(f32[2048]{0:T(1024)} %param.20) | copy-start | bytes 24580
Sparse Core Ops, SparseCore 0:
  9.6 42.3 all-gather.6
  54.3 38.2 all-gather.8
  94.1 57.5 all-gather.10
  153.9 93.9 all-gather.12
  250.0 92.2 all-gather.14
  344.3 95.1 all-gather.16
  453.4 15.6 reduce-scatter.1
where the time goes:
time: 479 us; the launch traced here: 478 us
  waiting for transfers between devices  362 us (76%)
  matrix products  46 us (10%)
  local copies, waits for them, and re-layouts  23.4 us (5%)
  blocking collectives  21.8 us (5%)
  between operations  13.7 us (3%)
  other arithmetic  10.2 us (2%)
    all_gather x1, waiting for transfers between devices, body(): lax.all_gather(w_down, 'sp', axis=1, tiled=True)  97.2 us
    all_gather x1, waiting for transfers between devices, body(): lax.all_gather(w_up, 'sp', axis=0, tiled=True)  86.4 us
    all_gather x1, waiting for transfers between devices, body(): lax.all_gather(w_gate, 'sp', axis=0, tiled=True)  81.3 us
    all_gather x1, waiting for transfers between devices, body(): key_piece = lax.all_gather(k_rot, 'sp', axis=0, tiled=True)  38.7 us
    all_gather x1, waiting for transfers between devices, body(): value_piece = lax.all_gather(values, 'sp', axis=0, tiled=True)  32.7 us
    reduce_scatter x1, waiting for transfers between devices, body(): lax.psum_scatter(terms.astype(jnp.bfloat16), 'tp', scatter_dimension=0, t...  15.8 us
    dot_general x1, matrix products, body(): jnp.dot(hidden, lax.all_gather(w_down, 'sp', axis=1, tiled=True), preferr...  13.9 us
    all_gather x1, blocking collectives, body(): gathered = lax.all_gather(normed, 'tp', axis=0, tiled=True)  11.5 us
  transfers between devices with their start and end apart: 7, of which 7 were waited for; matrix products, arithmetic and copies ran while one was open for 12% of the time, Pallas kernels for 0%

commit v1 on v0

--- a/solution.py
+++ b/solution.py
@@ -7,6 +7,22 @@
 GRID_W = 128
 EPS = 1e-06
 THETA = 10000.0
+
+
+def arrays_form(slab_in, on_dim):
+    shard_axis = "sp"
+    nodes = lax.axis_size(shard_axis)
+    main = slab_in
+    newest = [(h - 1, h) for h in range(1, nodes)] + [(nodes - 1, 0)]
+    rows = [main]
+    for _ in range(nodes - 1):
+        main = lax.ppermute(main, axis_name=shard_axis, perm=newest)
+        rows += [main]
+    block_next = jnp.concatenate([*reversed(rows)], axis=on_dim)
+    all_rows = jnp.roll(
+        block_next, (lax.axis_index(shard_axis) + 1) * main.shape[on_dim], axis=on_dim
+    )
+    return all_rows
 
 
 def turn_half(part, angle):
@@ -61,7 +77,7 @@
         jnp.zeros((kv_heads, q_group, tok_rows, head_size), jnp.float32),
     )
     running = start_state
-    key_piece = lax.all_gather(k_rot, "sp", axis=0, tiled=True)
+    key_piece = arrays_form(k_rot, 0)
     value_piece = lax.all_gather(values, "sp", axis=0, tiled=True)
     piece_len = key_piece.shape[0]
     block_len = math.gcd(piece_len, 512)

time: 479 us -> 439 us (0.916)
  waiting for transfers between devices: 362 us -> 321 us
    ppermute x0 -> x15, waiting for transfers between devices: none -> 107 us  [arrays_form(): main = lax.ppermute(main, axis_name=shard_axis, perm=newest)]
    all_gather x1, waiting for transfers between devices: 81.3 us -> 11.9 us  [body(): lax.all_gather(w_gate, 'sp', axis=0, tiled=True)]
    all_gather x1 -> x0, waiting for transfers between devices: 38.7 us -> none  [body(): key_piece = lax.all_gather(k_rot, 'sp', axis=0, tiled=True)]
    all_gather x1, waiting for transfers between devices: 32.7 us -> 0.01 us  [body(): value_piece = lax.all_gather(values, 'sp', axis=0, tiled=True)]
    all_gather x1, waiting for transfers between devices: 7.22 us -> 0.02 us  [body(): lax.all_gather(w_out, 'tp', axis=0, tiled=True)]
    concatenate x0 -> x1, local copies, waits for them, and re-layouts: none -> 6.27 us  [arrays_form(): jnp.roll(block_next, (lax.axis_index(shard_axis) + 1) * main.shape[on_dim...]
  transfers between devices with their start and end apart: 7 -> 21, of which waited for: 7 -> 19; matrix products, arithmetic and copies ran while one was open for 12% -> 14% of each run, Pallas kernels for 0% -> 0%
where the time goes in v1:
time: 439 us; the launch traced here: 438 us
  waiting for transfers between devices  321 us (73%)
  matrix products  46 us (10%)
  local copies, waits for them, and re-layouts  27.8 us (6%)
  blocking collectives  17.9 us (4%)
  between operations  13.9 us (3%)
  other arithmetic  9.56 us (2%)
    ppermute x15, waiting for transfers between devices, arrays_form(): main = lax.ppermute(main, axis_name=shard_axis, perm=newest)  107 us
    all_gather x1, waiting for transfers between devices, body(): lax.all_gather(w_down, 'sp', axis=1, tiled=True)  97.2 us
    all_gather x1, waiting for transfers between devices, body(): lax.all_gather(w_up, 'sp', axis=0, tiled=True)  86.4 us
    reduce_scatter x1, waiting for transfers between devices, body(): lax.psum_scatter(terms.astype(jnp.bfloat16), 'tp', scatter_dimension=0, t...  15.8 us
    dot_general x1, matrix products, body(): jnp.dot(hidden, lax.all_gather(w_down, 'sp', axis=1, tiled=True), preferr...  13.8 us
    all_gather x1, waiting for transfers between devices, body(): lax.all_gather(w_gate, 'sp', axis=0, tiled=True)  11.9 us
    dot_general x6, matrix products, update(): jnp.einsum('hgqk,khd->hgqd', weights.astype(jnp.bfloat16), value_block, p...  10.9 us
    dot_general x6, matrix products, update(): jnp.einsum('qhgd,khd->hgqk', query_groups, key_block, preferred_element_t...  10.1 us
  transfers between devices with their start and end apart: 21, of which 19 were waited for; matrix products, arithmetic and copies ran while one was open for 14% of the time, Pallas kernels for 0%

profile of v1, /device:TPU:0, one launch (start us, length us, event | category | flops | bytes accessed | tf_op | source)
XLA Modules:
  0.0 437.6 jit_solution(17263330878613538062)
XLA Ops:
  11.1 7.6 %collective-permute-done = bf16[192,256]{0,1:T(8,128)(2,1)S(1)} collective-permute-done((bf16[192,256]{0,1:T(8,128)(2,1)S(1)}, bf16[192,256]{0,1:T(8,128)(2,1)S(1)}, u32[]{:S(2)}, u32[]{:S(2)}) %collective-permute-start) | collective-permute-done | bytes 98336 | tf_op jit(solution)/shard_map/ppermute | solution.py:19
  18.8 7.3 %collective-permute-done.1 = bf16[192,256]{0,1:T(8,128)(2,1)S(1)} collective-permute-done((bf16[192,256]{0,1:T(8,128)(2,1)S(1)}, bf16[192,256]{0,1:T(8,128)(2,1)S(1)}, u32[]{:S(2)}, u32[]{:S(2)}) %collective-permute-start.1) | collective-permute-done | bytes 98336 | tf_op jit(solution)/shard_map/ppermute | solution.py:19
  26.0 7.3 %collective-permute-done.2 = bf16[192,256]{0,1:T(8,128)(2,1)S(1)} collective-permute-done((bf16[192,256]{0,1:T(8,128)(2,1)S(1)}, bf16[192,256]{0,1:T(8,128)(2,1)S(1)}, u32[]{:S(2)}, u32[]{:S(2)}) %collective-permute-start.2) | collective-permute-done | bytes 98336 | tf_op jit(solution)/shard_map/ppermute | solution.py:19
  33.4 7.1 %collective-permute-done.3 = bf16[192,256]{0,1:T(8,128)(2,1)S(1)} collective-permute-done((bf16[192,256]{0,1:T(8,128)(2,1)S(1)}, bf16[192,256]{0,1:T(8,128)(2,1)S(1)}, u32[]{:S(2)}, u32[]{:S(2)}) %collective-permute-start.3) | collective-permute-done | bytes 98336 | tf_op jit(solution)/shard_map/ppermute | solution.py:19
  40.5 7.6 %collective-permute-done.4 = bf16[192,256]{0,1:T(8,128)(2,1)S(1)} collective-permute-done((bf16[192,256]{0,1:T(8,128)(2,1)S(1)}, bf16[192,256]{0,1:T(8,128)(2,1)S(1)}, u32[]{:S(2)}, u32[]{:S(2)}) %collective-permute-start.4) | collective-permute-done | bytes 98336 | tf_op jit(solution)/shard_map/ppermute | solution.py:19
  48.2 7.1 %collective-permute-done.5 = bf16[192,256]{0,1:T(8,128)(2,1)S(1)} collective-permute-done((bf16[192,256]{0,1:T(8,128)(2,1)S(1)}, bf16[192,256]{0,1:T(8,128)(2,1)S(1)}, u32[]{:S(2)}, u32[]{:S(2)}) %collective-permute-start.5) | collective-permute-done | bytes 98336 | tf_op jit(solution)/shard_map/ppermute | solution.py:19
  55.3 7.1 %collective-permute-done.6 = bf16[192,256]{0,1:T(8,128)(2,1)S(1)} collective-permute-done((bf16[192,256]{0,1:T(8,128)(2,1)S(1)}, bf16[192,256]{0,1:T(8,128)(2,1)S(1)}, u32[]{:S(2)}, u32[]{:S(2)}) %collective-permute-start.6) | collective-permute-done | bytes 98336 | tf_op jit(solution)/shard_map/ppermute | solution.py:19
  62.3 7.1 %collective-permute-done.7 = bf16[192,256]{0,1:T(8,128)(2,1)S(1)} collective-permute-done((bf16[192,256]{0,1:T(8,128)(2,1)S(1)}, bf16[192,256]{0,1:T(8,128)(2,1)S(1)}, u32[]{:S(2)}, u32[]{:S(2)}) %collective-permute-start.7) | collective-permute-done | bytes 98336 | tf_op jit(solution)/shard_map/ppermute | solution.py:19
  69.4 7.1 %collective-permute-done.8 = bf16[192,256]{0,1:T(8,128)(2,1)S(1)} collective-permute-done((bf16[192,256]{0,1:T(8,128)(2,1)S(1)}, bf16[192,256]{0,1:T(8,128)(2,1)S(1)}, u32[]{:S(2)}, u32[]{:S(2)}) %collective-permute-start.8) | collective-permute-done | bytes 98336 | tf_op jit(solution)/shard_map/ppermute | solution.py:19
  76.8 6.9 %collective-permute-done.9 = bf16[192,256]{0,1:T(8,128)(2,1)S(1)} collective-permute-done((bf16[192,256]{0,1:T(8,128)(2,1)S(1)}, bf16[192,256]{0,1:T(8,128)(2,1)S(1)}, u32[]{:S(2)}, u32[]{:S(2)}) %collective-permute-start.9) | collective-permute-done | bytes 98336 | tf_op jit(solution)/shard_map/ppermute | solution.py:19
  83.8 7.0 %collective-permute-done.10 = bf16[192,256]{0,1:T(8,128)(2,1)S(1)} collective-permute-done((bf16[192,256]{0,1:T(8,128)(2,1)S(1)}, bf16[192,256]{0,1:T(8,128)(2,1)S(1)}, u32[]{:S(2)}, u32[]{:S(2)}) %collective-permute-start.10) | collective-permute-done | bytes 98336 | tf_op jit(solution)/shard_map/ppermute | solution.py:19
  90.8 7.1 %collective-permute-done.11 = bf16[192,256]{0,1:T(8,128)(2,1)S(1)} collective-permute-done((bf16[192,256]{0,1:T(8,128)(2,1)S(1)}, bf16[192,256]{0,1:T(8,128)(2,1)S(1)}, u32[]{:S(2)}, u32[]{:S(2)}) %collective-permute-start.11) | collective-permute-done | bytes 98336 | tf_op jit(solution)/shard_map/ppermute | solution.py:19
  98.0 7.0 %collective-permute-done.12 = bf16[192,256]{0,1:T(8,128)(2,1)S(1)} collective-permute-done((bf16[192,256]{0,1:T(8,128)(2,1)S(1)}, bf16[192,256]{0,1:T(8,128)(2,1)S(1)}, u32[]{:S(2)}, u32[]{:S(2)}) %collective-permute-start.12) | collective-permute-done | bytes 98336 | tf_op jit(solution)/shard_map/ppermute | solution.py:19
  105.2 6.9 %collective-permute-done.13 = bf16[192,256]{0,1:T(8,128)(2,1)S(1)} collective-permute-done((bf16[192,256]{0,1:T(8,128)(2,1)S(1)}, bf16[192,256]{0,1:T(8,128)(2,1)S(1)}, u32[]{:S(2)}, u32[]{:S(2)}) %collective-permute-start.13) | collective-permute-done | bytes 98336 | tf_op jit(solution)/shard_map/ppermute | solution.py:19
  112.8 6.5 %collective-permute-done.14 = bf16[192,256]{0,1:T(8,128)(2,1)} collective-permute-done((bf16[192,256]{0,1:T(8,128)(2,1)S(1)}, bf16[192,256]{0,1:T(8,128)(2,1)}, u32[]{:S(2)}, u32[]{:S(2)}) %collective-permute-start.14) | collective-permute-done | bytes 98336 | tf_op jit(solution)/shard_map/ppermute | solution.py:19
  119.3 6.3 %concatenate.15 = bf16[6144,256]{0,1:T(8,128)(2,1)S(1)} concatenate(bf16[192,256]{0,1:T(8,128)(2,1)} %collective-permute-done.14, bf16[192,256]{0,1:T(8,128)(2,1)} %copy-done.15, bf16[192,256]{0,1:T(8,128)(2,1)} %copy-done.14, bf16[192,256]{0,1:T(8,128)(2,1)} %copy-done.13, bf16[192,256]{0,1:T(8,128)(2,1)} %copy-done.12, bf16[192,256]{0,1:T(8,128)(2,1)} %copy-done.11, ...), dimensions={0} | concatenate | bytes 6291456 | tf_op jit(solution)/shard_map/jit(_roll_dynamic)/concatenate | solution.py:22
  125.6 1.8 constant_dynamic-slice_fusion
  127.4 3.4 reshape.197
  132.6 4.6 %reshape.207 = bf16[6,512,4,64]{3,2,1,0:T(4,128)(2,1)S(1)} reshape(bf16[3072,256]{1,0:T(8,128)(2,1)} %all-gather.6.cloned.1.call-done) | data formatting | bytes 3145728 | tf_op jit(solution)/shard_map/reshape | solution.py:86
  137.2 3.3 copy.27
  140.5 32.4 %while.15 = (s32[]{:T(128)}, f32[4,2,192]{2,1,0:T(2,128)S(1)}, f32[4,2,192]{2,1,0:T(2,128)S(1)}, f32[4,2,192,64]{2,3,1,0:T(8,128)}, bf16[6,512,4,64]{1,3,2,0:T(8...) while((s32[]{:T(128)}, f32[4,2,192]{2,1,0:T(2,128)S(1)}, ...), condition=%wide.region_5.6_spmd.clone, body=%wide.region_2.5_spmd.clone.sunk | while | flops 207920640 | bytes 14189729 | solution.py:109
  154.1 1.9 fusion.52
  174.3 9.3 %all_to_all.16 = bf16[2,96,512]{2,1,0:T(8,128)(2,1)S(1)} all-to-all(bf16[2,96,512]{2,1,0:T(8,128)(2,1)S(1)} %copy.28), channel_id=1, replica_groups=mesh['sp'=16,'tp'=2] {'tp'}, dimensions={0} | all-to-all | bytes 393216 | tf_op jit(solution)/shard_map/all_to_all | solution.py:117
  183.7 3.2 multiply_reduce_fusion
  187.0 8.6 %all_gather.20 = bf16[192,2048]{1,0:T(8,128)(2,1)S(1)} all-gather(bf16[96,2048]{1,0:T(8,128)(2,1)S(1)} %multiply_convert_fusion), channel_id=1, replica_groups=mesh['sp'=16,'tp'=2] {'tp'}, dimensions={0}, use_global_device_ids=true | all-gather | bytes 1179648 | tf_op jit(solution)/shard_map/all_gather | solution.py:126
  195.7 11.9 %all-gather.10.cloned.1.call-done = bf16[2048,2816]{1,0:T(8,128)(2,1)} async-done(((bf16[128,2816]{1,0:T(8,128)(2,1)}), bf16[2048,2816]{1,0:T(8,128)(2,1)}) %all-gather.10.cloned.1.call-update) | async-done | bytes 11534352 | tf_op jit(solution)/shard_map/all_gather | solution.py:130
  207.6 8.0 %fusion.30 = f32[192,2816]{1,0:T(8,128)} fusion(bf16[192,2048]{1,0:T(8,128)(2,1)S(1)} %all_gather.20, bf16[2048,2816]{1,0:T(8,128)(2,1)} %all-gather.10.cloned.1.call-done), kind=kOutput, calls=%fused_computation.70 | convolution fusion | flops 2214592512 | bytes 14483456 | tf_op jit(solution)/shard_map/dot_general | solution.py:128
  215.6 86.4 %all-gather.12.cloned.1.call-done = bf16[2048,2816]{1,0:T(8,128)(2,1)} async-done(((bf16[128,2816]{1,0:T(8,128)(2,1)}), bf16[2048,2816]{1,0:T(8,128)(2,1)}) %all-gather.12.cloned.1.call-update) | async-done | bytes 11534352 | tf_op jit(solution)/shard_map/all_gather | solution.py:134
  302.0 97.2 %all-gather.14.cloned.1.call-done = bf16[2816,2048]{1,0:T(8,128)(2,1)} async-done(((bf16[2816,128]{1,0:T(8,128)(2,1)}), bf16[2816,2048]{1,0:T(8,128)(2,1)}) %all-gather.14.cloned.1.call-update) | async-done | bytes 11534352 | tf_op jit(solution)/shard_map/all_gather | solution.py:138
  399.2 13.8 %convolution_convert_fusion = bf16[192,2048]{1,0:T(8,128)(2,1)} fusion(bf16[2816,2048]{1,0:T(8,128)(2,1)} %all-gather.14.cloned.1.call-done, bf16[192,2048]{1,0:T(8,128)(2,1)S(1)} %all_gather.20, bf16[2048,2816]{1,0:T(8,128)(2,1)} %all-gather.12.cloned.1.call-done, f32[192,2816]{1,0:T(8,128)} %fusion.30), kind=kOutput, calls=%fused_computation.25 | convolution fusion | flops 4432822272 | bytes 26804224 | tf_op jit(solution)/shard_map/dot_general | solution.py:137
  413.0 15.8 %reduce-scatter.2.cloned.1.call-done = bf16[96,2048]{1,0:T(8,128)(2,1)} async-done(((bf16[192,2048]{1,0:T(8,128)(2,1)}), bf16[96,2048]{1,0:T(8,128)(2,1)}) %reduce-scatter.2.cloned.1.call-update) | async-done | bytes 393232 | tf_op jit(solution)/shard_map/reduce_scatter | solution.py:140
  428.9 1.8 add_convert_fusion
  (151 shorter events, 39.1 us)
Async XLA Ops:
  6.5 70.1 %copy-start.16 = (bf16[192,512]{1,0:T(8,128)(2,1)S(1)}, bf16[192,512]{1,0:T(8,128)(2,1)}, u32[]{:S(2)}) copy-start(bf16[192,512]{1,0:T(8,128)(2,1)} %param.13) | copy-start | bytes 589828
  6.5 126.0 %all-gather.6.cloned.1.call-start = ((), (), s32[]{:S(2)}) async-start(), calls=%async_computation.2 | async-start | bytes 1671168 | tf_op jit(solution)/shard_map/all_gather | solution.py:81
  7.3 90.7 %copy-start.20 = (f32[64]{0:T(128)S(1)}, f32[64]{0:T(128)}, u32[]{:S(2)}) copy-start(f32[64]{0:T(128)} %param.16) | copy-start | bytes 772
  7.3 176.4 %all-gather.8.cloned.1.call-start = ((), (), s32[]{:S(2)}) async-start(), calls=%async_computation.3 | async-start | bytes 6291456 | tf_op jit(solution)/shard_map/all_gather | solution.py:120
  8.0 199.6 %all-gather.10.cloned.1.call-start = ((), (), s32[]{:S(2)}) async-start(), calls=%async_computation.4 | async-start | bytes 12255232 | tf_op jit(solution)/shard_map/all_gather | solution.py:130
  8.8 293.2 %all-gather.12.cloned.1.call-start = ((), (), s32[]{:S(2)}) async-start(), calls=%async_computation.5 | async-start | bytes 12255232 | tf_op jit(solution)/shard_map/all_gather | solution.py:134
  9.3 389.8 %all-gather.14.cloned.1.call-start = ((), (), s32[]{:S(2)}) async-start(), calls=%async_computation.6 | async-start | bytes 12255232 | tf_op jit(solution)/shard_map/all_gather | solution.py:138
  9.9 418.9 %reduce-scatter.2.cloned.1.call-start = ((), (), s32[]{:S(2)}) async-start(), calls=%async_computation.7 | async-start | bytes 1179648 | tf_op jit(solution)/shard_map/reduce_scatter | solution.py:140
  10.6 8.2 %collective-permute-start = (bf16[192,256]{0,1:T(8,128)(2,1)S(1)}, bf16[192,256]{0,1:T(8,128)(2,1)S(1)}, u32[]{:S(2)}, u32[]{:S(2)}) collective-permute-start(bf16[192,256]{0,1:T(8,128)(2,1)S(1)} %bitcast.68), channel_id=1, source_target_pairs={{0,2},{2,4},{4,6},{6,8},{8,10},{10,12},{12,14},{14,16},{16,18},{18... | collective-permute-start | bytes 294920 | tf_op jit(solution)/shard_map/ppermute | solution.py:19
  18.7 57.8 %copy-start.2 = (bf16[192,256]{0,1:T(8,128)(2,1)}, bf16[192,256]{0,1:T(8,128)(2,1)S(1)}, u32[]{:S(2)}) copy-start(bf16[192,256]{0,1:T(8,128)(2,1)S(1)} %collective-permute-done) | copy-start | bytes 294916
  18.7 7.3 %collective-permute-start.1 = (bf16[192,256]{0,1:T(8,128)(2,1)S(1)}, bf16[192,256]{0,1:T(8,128)(2,1)S(1)}, u32[]{:S(2)}, u32[]{:S(2)}) collective-permute-start(bf16[192,256]{0,1:T(8,128)(2,1)S(1)} %collective-permute-done), channel_id=1, source_target_pairs={{0,2},{2,4},{4,6},{6,8},{8,10},{10,12},{12,14},{14,16},{16,18},{18... | collective-permute-start | bytes 294920 | tf_op jit(solution)/shard_map/ppermute | solution.py:19
  26.0 50.5 %copy-start.3 = (bf16[192,256]{0,1:T(8,128)(2,1)}, bf16[192,256]{0,1:T(8,128)(2,1)S(1)}, u32[]{:S(2)}) copy-start(bf16[192,256]{0,1:T(8,128)(2,1)S(1)} %collective-permute-done.1) | copy-start | bytes 294916
  26.0 7.3 %collective-permute-start.2 = (bf16[192,256]{0,1:T(8,128)(2,1)S(1)}, bf16[192,256]{0,1:T(8,128)(2,1)S(1)}, u32[]{:S(2)}, u32[]{:S(2)}) collective-permute-start(bf16[192,256]{0,1:T(8,128)(2,1)S(1)} %collective-permute-done.1), channel_id=1, source_target_pairs={{0,2},{2,4},{4,6},{6,8},{8,10},{10,12},{12,14},{14,16},{16,18},{18... | collective-permute-start | bytes 294920 | tf_op jit(solution)/shard_map/ppermute | solution.py:19
  33.4 43.2 %copy-start.4 = (bf16[192,256]{0,1:T(8,128)(2,1)}, bf16[192,256]{0,1:T(8,128)(2,1)S(1)}, u32[]{:S(2)}) copy-start(bf16[192,256]{0,1:T(8,128)(2,1)S(1)} %collective-permute-done.2) | copy-start | bytes 294916
  33.4 7.1 %collective-permute-start.3 = (bf16[192,256]{0,1:T(8,128)(2,1)S(1)}, bf16[192,256]{0,1:T(8,128)(2,1)S(1)}, u32[]{:S(2)}, u32[]{:S(2)}) collective-permute-start(bf16[192,256]{0,1:T(8,128)(2,1)S(1)} %collective-permute-done.2), channel_id=1, source_target_pairs={{0,2},{2,4},{4,6},{6,8},{8,10},{10,12},{12,14},{14,16},{16,18},{18... | collective-permute-start | bytes 294920 | tf_op jit(solution)/shard_map/ppermute | solution.py:19
  40.5 36.0 %copy-start.5 = (bf16[192,256]{0,1:T(8,128)(2,1)}, bf16[192,256]{0,1:T(8,128)(2,1)S(1)}, u32[]{:S(2)}) copy-start(bf16[192,256]{0,1:T(8,128)(2,1)S(1)} %collective-permute-done.3) | copy-start | bytes 294916
  40.5 7.7 %collective-permute-start.4 = (bf16[192,256]{0,1:T(8,128)(2,1)S(1)}, bf16[192,256]{0,1:T(8,128)(2,1)S(1)}, u32[]{:S(2)}, u32[]{:S(2)}) collective-permute-start(bf16[192,256]{0,1:T(8,128)(2,1)S(1)} %collective-permute-done.3), channel_id=1, source_target_pairs={{0,2},{2,4},{4,6},{6,8},{8,10},{10,12},{12,14},{14,16},{16,18},{18... | collective-permute-start | bytes 294920 | tf_op jit(solution)/shard_map/ppermute | solution.py:19
  48.2 28.4 %copy-start.6 = (bf16[192,256]{0,1:T(8,128)(2,1)}, bf16[192,256]{0,1:T(8,128)(2,1)S(1)}, u32[]{:S(2)}) copy-start(bf16[192,256]{0,1:T(8,128)(2,1)S(1)} %collective-permute-done.4) | copy-start | bytes 294916
  48.2 7.1 %collective-permute-start.5 = (bf16[192,256]{0,1:T(8,128)(2,1)S(1)}, bf16[192,256]{0,1:T(8,128)(2,1)S(1)}, u32[]{:S(2)}, u32[]{:S(2)}) collective-permute-start(bf16[192,256]{0,1:T(8,128)(2,1)S(1)} %collective-permute-done.4), channel_id=1, source_target_pairs={{0,2},{2,4},{4,6},{6,8},{8,10},{10,12},{12,14},{14,16},{16,18},{18... | collective-permute-start | bytes 294920 | tf_op jit(solution)/shard_map/ppermute | solution.py:19
  55.2 21.3 %copy-start.7 = (bf16[192,256]{0,1:T(8,128)(2,1)}, bf16[192,256]{0,1:T(8,128)(2,1)S(1)}, u32[]{:S(2)}) copy-start(bf16[192,256]{0,1:T(8,128)(2,1)S(1)} %collective-permute-done.5) | copy-start | bytes 294916
  55.2 7.1 %collective-permute-start.6 = (bf16[192,256]{0,1:T(8,128)(2,1)S(1)}, bf16[192,256]{0,1:T(8,128)(2,1)S(1)}, u32[]{:S(2)}, u32[]{:S(2)}) collective-permute-start(bf16[192,256]{0,1:T(8,128)(2,1)S(1)} %collective-permute-done.5), channel_id=1, source_target_pairs={{0,2},{2,4},{4,6},{6,8},{8,10},{10,12},{12,14},{14,16},{16,18},{18... | collective-permute-start | bytes 294920 | tf_op jit(solution)/shard_map/ppermute | solution.py:19
  62.3 7.1 %collective-permute-start.7 = (bf16[192,256]{0,1:T(8,128)(2,1)S(1)}, bf16[192,256]{0,1:T(8,128)(2,1)S(1)}, u32[]{:S(2)}, u32[]{:S(2)}) collective-permute-start(bf16[192,256]{0,1:T(8,128)(2,1)S(1)} %collective-permute-done.6), channel_id=1, source_target_pairs={{0,2},{2,4},{4,6},{6,8},{8,10},{10,12},{12,14},{14,16},{16,18},{18... | collective-permute-start | bytes 294920 | tf_op jit(solution)/shard_map/ppermute | solution.py:19
  69.4 7.1 %collective-permute-start.8 = (bf16[192,256]{0,1:T(8,128)(2,1)S(1)}, bf16[192,256]{0,1:T(8,128)(2,1)S(1)}, u32[]{:S(2)}, u32[]{:S(2)}) collective-permute-start(bf16[192,256]{0,1:T(8,128)(2,1)S(1)} %collective-permute-done.7), channel_id=1, source_target_pairs={{0,2},{2,4},{4,6},{6,8},{8,10},{10,12},{12,14},{14,16},{16,18},{18... | collective-permute-start | bytes 294920 | tf_op jit(solution)/shard_map/ppermute | solution.py:19
  76.6 35.6 %copy-start.10 = (bf16[192,256]{0,1:T(8,128)(2,1)}, bf16[192,256]{0,1:T(8,128)(2,1)S(1)}, u32[]{:S(2)}) copy-start(bf16[192,256]{0,1:T(8,128)(2,1)S(1)} %collective-permute-done.8) | copy-start | bytes 294916
  76.6 7.1 %collective-permute-start.9 = (bf16[192,256]{0,1:T(8,128)(2,1)S(1)}, bf16[192,256]{0,1:T(8,128)(2,1)S(1)}, u32[]{:S(2)}, u32[]{:S(2)}) collective-permute-start(bf16[192,256]{0,1:T(8,128)(2,1)S(1)} %collective-permute-done.8), channel_id=1, source_target_pairs={{0,2},{2,4},{4,6},{6,8},{8,10},{10,12},{12,14},{14,16},{16,18},{18... | collective-permute-start | bytes 294920 | tf_op jit(solution)/shard_map/ppermute | solution.py:19
  83.7 28.4 %copy-start.11 = (bf16[192,256]{0,1:T(8,128)(2,1)}, bf16[192,256]{0,1:T(8,128)(2,1)S(1)}, u32[]{:S(2)}) copy-start(bf16[192,256]{0,1:T(8,128)(2,1)S(1)} %collective-permute-done.9) | copy-start | bytes 294916
  83.7 7.1 %collective-permute-start.10 = (bf16[192,256]{0,1:T(8,128)(2,1)S(1)}, bf16[192,256]{0,1:T(8,128)(2,1)S(1)}, u32[]{:S(2)}, u32[]{:S(2)}) collective-permute-start(bf16[192,256]{0,1:T(8,128)(2,1)S(1)} %collective-permute-done.9), channel_id=1, source_target_pairs={{0,2},{2,4},{4,6},{6,8},{8,10},{10,12},{12,14},{14,16},{16,18},{18... | collective-permute-start | bytes 294920 | tf_op jit(solution)/shard_map/ppermute | solution.py:19
  90.8 21.3 %copy-start.12 = (bf16[192,256]{0,1:T(8,128)(2,1)}, bf16[192,256]{0,1:T(8,128)(2,1)S(1)}, u32[]{:S(2)}) copy-start(bf16[192,256]{0,1:T(8,128)(2,1)S(1)} %collective-permute-done.10) | copy-start | bytes 294916
  90.8 7.1 %collective-permute-start.11 = (bf16[192,256]{0,1:T(8,128)(2,1)S(1)}, bf16[192,256]{0,1:T(8,128)(2,1)S(1)}, u32[]{:S(2)}, u32[]{:S(2)}) collective-permute-start(bf16[192,256]{0,1:T(8,128)(2,1)S(1)} %collective-permute-done.10), channel_id=1, source_target_pairs={{0,2},{2,4},{4,6},{6,8},{8,10},{10,12},{12,14},{14,16},{16,18},{18... | collective-permute-start | bytes 294920 | tf_op jit(solution)/shard_map/ppermute | solution.py:19
  97.9 7.1 %collective-permute-start.12 = (bf16[192,256]{0,1:T(8,128)(2,1)S(1)}, bf16[192,256]{0,1:T(8,128)(2,1)S(1)}, u32[]{:S(2)}, u32[]{:S(2)}) collective-permute-start(bf16[192,256]{0,1:T(8,128)(2,1)S(1)} %collective-permute-done.11), channel_id=1, source_target_pairs={{0,2},{2,4},{4,6},{6,8},{8,10},{10,12},{12,14},{14,16},{16,18},{18... | collective-permute-start | bytes 294920 | tf_op jit(solution)/shard_map/ppermute | solution.py:19
  105.0 7.1 %collective-permute-start.13 = (bf16[192,256]{0,1:T(8,128)(2,1)S(1)}, bf16[192,256]{0,1:T(8,128)(2,1)S(1)}, u32[]{:S(2)}, u32[]{:S(2)}) collective-permute-start(bf16[192,256]{0,1:T(8,128)(2,1)S(1)} %collective-permute-done.12), channel_id=1, source_target_pairs={{0,2},{2,4},{4,6},{6,8},{8,10},{10,12},{12,14},{14,16},{16,18},{18... | collective-permute-start | bytes 294920 | tf_op jit(solution)/shard_map/ppermute | solution.py:19
  112.1 7.2 %collective-permute-start.14 = (bf16[192,256]{0,1:T(8,128)(2,1)S(1)}, bf16[192,256]{0,1:T(8,128)(2,1)}, u32[]{:S(2)}, u32[]{:S(2)}) collective-permute-start(bf16[192,256]{0,1:T(8,128)(2,1)S(1)} %collective-permute-done.13), channel_id=1, source_target_pairs={{0,2},{2,4},{4,6},{6,8},{8,10},{10,12},{12,14},{14,16},{16,18},{18... | collective-permute-start | bytes 294920 | tf_op jit(solution)/shard_map/ppermute | solution.py:19
  (20 other events, 74.6 us)
Sparse Core Ops, SparseCore 0:
  9.6 43.8 all-gather.5
  55.1 56.1 all-gather.7
  113.5 94.0 all-gather.9
  209.7 92.2 all-gather.11
  304.0 95.1 all-gather.13
  413.1 15.6 reduce-scatter.1
